TPU v7x, 32 devices: a whole 2x2x4 slice. The times are simulated.
32 devices in a mesh: grp: 2 (over x), ep: 16 (over z, y, core).
Axes of the slice: x: 2, y: 2, z: 4, core: 2. Of those that a mesh axis runs over, the one named last changes fastest.
Arguments:
- tokens: bfloat16 [256, 2048], P(('grp', 'ep')), parts along dimension 0, may hold values from -6 to 6
- state: float32 [256, 8, 64, 128], P(('grp', 'ep')), parts along dimension 0, may hold values from -6 to 6
- g_mix: float32 [2048], replicated, may hold values from 0.1 to 1.9
- w_query: bfloat16 [2048, 512], P('ep'), may hold values from -0.125 to 0.125
- w_key: bfloat16 [2048, 512], P('ep'), may hold values from -0.125 to 0.125
- w_value: bfloat16 [2048, 1024], P('ep'), may hold values from -0.125 to 0.125
- w_decay_down: bfloat16 [2048, 32], replicated, may hold values from -0.125 to 0.125
- w_decay_up: bfloat16 [32, 512], replicated, may hold values from -1 to 1
- decay_bias: float32 [512], replicated, may hold values from -6 to 2
- g_head: float32 [128], replicated, may hold values from 0.1 to 1.9
- w_out: bfloat16 [1024, 2048], replicated, may hold values from -0.1875 to 0.1875
- g_ffn: float32 [2048], replicated, may hold values from 0.1 to 1.9
- routes: int32 [256, 4], P(('grp', 'ep')), parts along dimension 0, may hold values from 0 to 31, all different within a row; in each aligned block of 8 rows (0 to 7, 8 to 15, ...) at most 2 rows name the same one
- route_scores: float32 [256, 4], P(('grp', 'ep')), parts along dimension 0, may hold values from -9 to 320
- w_gate_in: bfloat16 [32, 2048, 1024], P('ep'), may hold values from -0.375 to 0.375
- w_lin_in: bfloat16 [32, 2048, 1024], P('ep'), may hold values from -0.375 to 0.375
- w_down: bfloat16 [32, 1024, 2048], P('ep'), may hold values from -0.046875 to 0.046875
Outputs:
- output: bfloat16 [256, 2048], P(('grp', 'ep')), parts along dimension 0
- new_state: float32 [256, 8, 64, 128], P(('grp', 'ep')), parts along dimension 0
There are 2 independent parts, one for each index of `grp`. A program takes and returns all parts, laid end to end along the dimension named above; an argument that names none is the same for every part. Nothing has to cross between parts.
Inputs may be any that keep to these rules, and one draw needn't show every extreme that they name: `routes`: each row names 4 different experts; the rows of one device name no expert more than 2 times, a bound that some block reaches.
All inputs are finite; a program needn't handle non-finite values.
Results may differ from a plain program's by a relative error of at most 0.014.
Values may be sent and summed in bfloat16 or wider, within the bound.
A program may use at most 128 MiB of HBM per device.

v0:
```python
import jax
import jax.numpy as jnp
from jax import lax
from jax.sharding import PartitionSpec as P

HEADS = 8
DK = 64
DV = 128
EXPERTS = 32
CAP = 2


EPS = 1e-06
TAU = 16.0
ALPHA = 1.702
LIMIT = 7.0


def rms_scale(values, gain):
    return values * lax.rsqrt(jnp.mean(values * values, axis=-1, keepdims=True) + EPS) * gain


def per_device(
    tokens,
    state,
    g_mix,
    w_query,
    w_key,
    w_value,
    w_decay_down,
    w_decay_up,
    decay_bias,
    g_head,
    w_out,
    g_ffn,
    routes,
    route_scores,
    w_gate_in,
    w_lin_in,
    w_down,
):
    seq_rows = tokens.shape[0]
    query_width = w_query.shape[1]
    residual_in = tokens.astype(jnp.float32)
    normed = rms_scale(residual_in, g_mix).astype(jnp.bfloat16)
    joined = jnp.concatenate([w_query, w_key, w_value], axis=1)
    column_block = lax.all_to_all(joined, "ep", split_axis=1, concat_axis=0, tiled=True)
    all_columns = jnp.dot(
        lax.all_gather(normed, "ep", axis=0, tiled=True),
        column_block,
        preferred_element_type=jnp.float32,
    )
    summed = lax.all_to_all(all_columns, "ep", split_axis=0, concat_axis=1, tiled=True)
    query_flat = summed[:, :query_width]
    key_flat = summed[:, query_width : 2 * query_width]
    value_flat = summed[:, 2 * query_width :]
    queries = query_flat.reshape(seq_rows, HEADS, DK) * DK ** (-0.5)
    key_rows = key_flat.reshape(seq_rows, HEADS, DK)
    value_rows = value_flat.reshape(seq_rows, HEADS, DV)
    low_rank = jnp.dot(normed, w_decay_down, preferred_element_type=jnp.float32).astype(
        jnp.bfloat16
    )
    log_decay = (
        jax.nn.log_sigmoid(
            jnp.dot(low_rank, w_decay_up, preferred_element_type=jnp.float32) + decay_bias
        )
        / TAU
    )
    log_decay = log_decay.reshape(seq_rows, HEADS, DK)
    new_state = (
        jnp.exp(log_decay)[..., None] * state + key_rows[..., None] * value_rows[:, :, None, :]
    )
    attended = jnp.einsum("bhk,bhkv->bhv", queries, new_state, precision=lax.Precision.HIGHEST)
    headed = rms_scale(attended, g_head).astype(jnp.bfloat16).reshape(seq_rows, HEADS * DV)
    residual = (residual_in + jnp.dot(headed, w_out, preferred_element_type=jnp.float32)).astype(
        jnp.bfloat16
    )
    fed = rms_scale(residual.astype(jnp.float32), g_ffn).astype(jnp.bfloat16)
    top_count = routes.shape[1]
    slot_count = seq_rows * top_count
    slot_expert = routes.reshape(slot_count)
    slot_order = jnp.arange(slot_count, dtype=jnp.int32)
    earlier = (slot_expert[:, None] == slot_expert[None, :]) & (
        slot_order[None, :] < slot_order[:, None]
    )
    slot_rank = jnp.sum(earlier.astype(jnp.int32), axis=1)
    slot_dest = slot_expert * CAP + slot_rank
    slot_pick = (slot_dest[:, None] == jnp.arange(EXPERTS * CAP, dtype=jnp.int32)[None, :]).astype(
        jnp.bfloat16
    )
    token_pick = jnp.sum(slot_pick.reshape(seq_rows, top_count, EXPERTS * CAP), axis=1)
    outgoing = jnp.einsum("tx,td->xd", token_pick, fed, preferred_element_type=jnp.float32).astype(
        jnp.bfloat16
    )
    arrived = lax.all_to_all(outgoing, "ep", split_axis=0, concat_axis=0, tiled=True)
    local_experts = w_gate_in.shape[0]
    arrived = arrived.reshape(-1, local_experts, CAP, arrived.shape[1])
    gate_pre = jnp.minimum(
        jnp.einsum("secd,edf->secf", arrived, w_gate_in, preferred_element_type=jnp.float32), LIMIT
    )
    lin_pre = jnp.clip(
        jnp.einsum("secd,edf->secf", arrived, w_lin_in, preferred_element_type=jnp.float32),
        -LIMIT,
        LIMIT,
    )
    hidden = (gate_pre * jax.nn.sigmoid(ALPHA * gate_pre) * (lin_pre + 1.0)).astype(jnp.bfloat16)
    expert_out = jnp.einsum(
        "secf,efd->secd", hidden, w_down, preferred_element_type=jnp.float32
    ).astype(jnp.bfloat16)
    expert_out = expert_out.reshape(-1, expert_out.shape[3])
    returned = lax.all_to_all(expert_out, "ep", split_axis=0, concat_axis=0, tiled=True)
    gathered = jnp.einsum("sx,xd->sd", slot_pick, returned, preferred_element_type=jnp.float32)
    gathered = gathered.reshape(seq_rows, top_count, gathered.shape[1])
    weights = jax.nn.softmax(route_scores, axis=-1)
    expert_sum = jnp.sum(weights[..., None] * gathered, axis=1)
    output = (residual.astype(jnp.float32) + expert_sum).astype(jnp.bfloat16)
    return (output, new_state)


def solution(mesh):
    return jax.shard_map(
        per_device,
        mesh=mesh,
        in_specs=(
            P(("grp", "ep"), None),
            P(("grp", "ep"), None, None, None),
            P(),
            P("ep", None),
            P("ep", None),
            P("ep", None),
            P(),
            P(),
            P(),
            P(),
            P(),
            P(),
            P(("grp", "ep"), None),
            P(("grp", "ep"), None),
            P("ep", None, None),
            P("ep", None, None),
            P("ep", None, None),
        ),
        out_specs=(P(("grp", "ep"), None), P(("grp", "ep"), None, None, None)),
        check_vma=False,
    )
```

profile of v0, /device:TPU:0, one launch (start us, length us, event | category | flops | bytes accessed | tf_op | source)
XLA Modules:
  0.0 96.4 jit_solution(1850943474575072687)
XLA Ops:
  0.6 2.0 %copy_bitcast_fusion = bf16[128,16,128]{2,0,1:T(8,128)(2,1)} fusion(bf16[128,1024]{1,0:T(8,128)(2,1)} %param.22, bf16[128,512]{1,0:T(8,128)(2,1)} %param.21, bf16[128,512]{1,0:T(8,128)(2,1)} %param.20), kind=kLoop, calls=%fused_computation.24 | loop fusion | flops 1572864 | bytes 1048576 | tf_op jit(solution)/shard_map/all_to_all | solution.py:47
  2.7 7.4 %all-to-all-start = ((bf16[128,16,128]{2,0,1:T(8,128)(2,1)}), bf16[128,16,128]{2,0,1:T(8,128)(2,1)S(1)}, u32[]{:S(2)}, u32[]{:S(2)}) async-start(bf16[128,16,128]{2,0,1:T(8,128)(2,1)} %copy_bitcast_fusion), calls=%async_computation | async-start | bytes 1048576 | tf_op jit(solution)/shard_map/all_to_all | solution.py:47
  10.1 0.9 fusion.38
  11.0 0.8 copy.38
  11.8 0.2 convert_reduce_fusion
  12.1 0.8 fusion.40
  12.9 1.1 %fusion.46 = f32[8,512]{1,0:T(8,128)S(1)} fusion(bf16[32,512]{1,0:T(8,128)(2,1)} %param.24, bf16[8,2048]{1,0:T(8,128)(2,1)S(1)} %fusion.40, bf16[2048,32]{0,1:T(8,128)(2,1)S(1)} %copy-done, f32[512]{0:T(512)} %param.25), kind=kOutput, calls=%fused_computation.46 | convolution fusion | flops 1351936 | bytes 215040 | tf_op jit(solution)/shard_map/dot_general | solution.py:65
  14.0 23.2 %all_gather.3 = bf16[128,2048]{1,0:T(8,128)(2,1)S(1)} all-gather(bf16[8,2048]{1,0:T(8,128)(2,1)S(1)} %fusion.40), channel_id=1, replica_groups=mesh['grp'=2,'ep'=16] {'ep'}, dimensions={0}, use_global_device_ids=true | all-gather | bytes 557056 | tf_op jit(solution)/shard_map/all_gather | solution.py:49
  37.2 0.9 fusion.34
  38.1 3.5 %all-to-all-start.1 = ((f32[16,8,128]{2,1,0:T(8,128)}), f32[16,8,128]{2,1,0:T(8,128)S(1)}, u32[]{:S(2)}, u32[]{:S(2)}) async-start(f32[16,8,128]{2,1,0:T(8,128)} %fusion.34), calls=%async_computation.1 | async-start | bytes 131072 | tf_op jit(solution)/shard_map/all_to_all | solution.py:53
  41.9 6.6 %all-to-all-done.1 = f32[16,8,128]{2,1,0:T(8,128)S(1)} async-done(((f32[16,8,128]{2,1,0:T(8,128)}), f32[16,8,128]{2,1,0:T(8,128)S(1)}, u32[]{:S(2)}, u32[]{:S(2)}) %all-to-all-start.1) | async-done | bytes 65568 | tf_op jit(solution)/shard_map/all_to_all | solution.py:53
  48.6 2.6 %multiply_add_fusion = f32[8,8,64,128]{3,2,1,0:T(8,128)S(1)} fusion(f32[8,8,64,128]{3,2,1,0:T(8,128)} %param.18, f32[8,8,128]{2,1,0:T(8,128)S(1)} %bitcast.100, f32[8,8,64]{2,1,0:T(8,128)S(1)} %mul.131, f32[8,8,64]{2,1,0:T(8,128)S(1)} %exp.23), kind=kLoop, calls=%fused_computation.12 | loop fusion | flops 1572864 | bytes 4259840 | tf_op jit(solution)/shard_map/add | solution.py:71
  51.3 1.9 %fusion.62 = f32[8,8,1,128]{3,2,1,0:T(1,128)S(1)} fusion(f32[8,8,64,1]{2,3,1,0:T(1,128)S(1)} %bitcast.101, f32[8,8,64,128]{3,2,1,0:T(8,128)S(1)} %multiply_add_fusion), kind=kOutput, calls=%fused_computation.71 | convolution fusion | flops 6291456 | bytes 2146304 | tf_op jit(solution)/shard_map/bhk,bhkv->bhv/dot_general | solution.py:73
  53.3 0.8 multiply_reduce_fusion
  54.1 0.3 convolution_convert_fusion
  54.5 12.6 %all_to_all.56 = bf16[16,4,2048]{2,1,0:T(4,128)(2,1)S(1)} all-to-all(bf16[16,4,2048]{2,1,0:T(4,128)(2,1)S(1)} %all_to_all.47), channel_id=1, replica_groups=mesh['grp'=2,'ep'=16] {'ep'}, dimensions={0} | all-to-all | bytes 524288 | tf_op jit(solution)/shard_map/all_to_all | solution.py:95
  67.2 0.1 copy.42
  67.3 4.9 %fusion.14 = f32[16,2,2,1024]{3,0,2,1:T(8,128)S(1)} fusion(bf16[16,2,2,2048]{3,0,2,1:T(8,128)(2,1)S(1)} %bitcast.92, bf16[2,2048,1024]{2,1,0:T(8,128)(2,1)} %param.31), kind=kOutput, calls=%fused_computation.14 | convolution fusion | flops 268500992 | bytes 8912896 | tf_op jit(solution)/shard_map/secd,edf->secf/dot_general | solution.py:99
  72.3 8.8 %fusion.6 = bf16[2,16,2,2048]{3,1,2,0:T(8,128)(2,1)S(1)} fusion(bf16[2,1024,2048]{2,1,0:T(8,128)(2,1)} %param.33, bf16[16,2,2,2048]{3,0,2,1:T(8,128)(2,1)S(1)} %bitcast.93, bf16[2,2048,1024]{2,1,0:T(8,128)(2,1)} %param.32, f32[16,2,2,1024]{3,0,2,1:T(8,128)S(1)} %fusion.14), kind=kOutput, calls=%fused_computation.6 | convolution fusion | flops 537591808 | bytes 17563648 | tf_op jit(solution)/shard_map/secf,efd->secd/dot_general | solution.py:107
  81.0 0.9 copy.43
  81.9 3.5 %all-to-all-start.3 = ((bf16[16,4,2048]{2,1,0:T(4,128)(2,1)}), bf16[16,4,2048]{2,1,0:T(4,128)(2,1)S(1)}, u32[]{:S(2)}, u32[]{:S(2)}) async-start(bf16[16,4,2048]{2,1,0:T(4,128)(2,1)} %copy.43), calls=%async_computation.3 | async-start | bytes 524288 | tf_op jit(solution)/shard_map/all_to_all | solution.py:111
  85.5 9.9 %all-to-all-done.3 = bf16[16,4,2048]{2,1,0:T(4,128)(2,1)S(1)} async-done(((bf16[16,4,2048]{2,1,0:T(4,128)(2,1)}), bf16[16,4,2048]{2,1,0:T(4,128)(2,1)S(1)}, u32[]{:S(2)}, u32[]{:S(2)}) %all-to-all-start.3) | async-done | bytes 262176 | tf_op jit(solution)/shard_map/all_to_all | solution.py:111
  95.5 0.2 fusion.32
  95.8 0.6 add_convert_fusion
  (36 shorter events, 1.0 us)
Async XLA Ops:
  0.6 12.3 %copy-start = (bf16[2048,32]{0,1:T(8,128)(2,1)S(1)}, bf16[2048,32]{0,1:T(8,128)(2,1)}, u32[]{:S(2)}) copy-start(bf16[2048,32]{0,1:T(8,128)(2,1)} %param.23) | copy-start | bytes 393220
  2.7 34.5 %all-to-all-start = ((bf16[128,16,128]{2,0,1:T(8,128)(2,1)}), bf16[128,16,128]{2,0,1:T(8,128)(2,1)S(1)}, u32[]{:S(2)}, u32[]{:S(2)}) async-start(bf16[128,16,128]{2,0,1:T(8,128)(2,1)} %copy_bitcast_fusion), calls=%async_computation | async-start | bytes 1048576 | tf_op jit(solution)/shard_map/all_to_all | solution.py:47
  37.2 16.1 %copy-start.6 = (f32[128]{0:T(128)S(1)}, f32[128]{0:T(128)}, u32[]{:S(2)}) copy-start(f32[128]{0:T(128)} %param.26) | copy-start | bytes 1540
  37.2 16.2 %copy-start.3 = (bf16[8,2048]{1,0:T(8,128)(2,1)S(1)}, bf16[8,2048]{1,0:T(8,128)(2,1)}, u32[]{:S(2)}) copy-start(bf16[8,2048]{1,0:T(8,128)(2,1)} %param.17) | copy-start | bytes 98308
  38.1 10.4 %all-to-all-start.1 = ((f32[16,8,128]{2,1,0:T(8,128)}), f32[16,8,128]{2,1,0:T(8,128)S(1)}, u32[]{:S(2)}, u32[]{:S(2)}) async-start(f32[16,8,128]{2,1,0:T(8,128)} %fusion.34), calls=%async_computation.1 | async-start | bytes 131072 | tf_op jit(solution)/shard_map/all_to_all | solution.py:53
  48.6 4.7 %copy-start.2 = (bf16[1024,2048]{1,0:T(8,128)(2,1)S(1)}, bf16[1024,2048]{1,0:T(8,128)(2,1)}, u32[]{:S(2)}) copy-start(bf16[1024,2048]{1,0:T(8,128)(2,1)} %param.27) | copy-start | bytes 12582916
  51.3 16.0 %copy-start.1 = (f32[8,8,64,128]{3,2,1,0:T(8,128)}, f32[8,8,64,128]{3,2,1,0:T(8,128)S(1)}, u32[]{:S(2)}) copy-start(f32[8,8,64,128]{3,2,1,0:T(8,128)S(1)} %multiply_add_fusion) | copy-start | bytes 6291460
  51.3 2.9 %copy-start.5 = (f32[2048]{0:T(1024)S(1)}, f32[2048]{0:T(1024)}, u32[]{:S(2)}) copy-start(f32[2048]{0:T(1024)} %param.28) | copy-start | bytes 24580
  72.2 13.2 %copy-start.4 = (f32[8,4]{0,1:T(4,128)S(1)}, f32[8,4]{0,1:T(4,128)}, u32[]{:S(2)}) copy-start(f32[8,4]{0,1:T(4,128)} %param.30) | copy-start | bytes 388
  81.9 13.5 %all-to-all-start.3 = ((bf16[16,4,2048]{2,1,0:T(4,128)(2,1)}), bf16[16,4,2048]{2,1,0:T(4,128)(2,1)S(1)}, u32[]{:S(2)}, u32[]{:S(2)}) async-start(bf16[16,4,2048]{2,1,0:T(4,128)(2,1)} %copy.43), calls=%async_computation.3 | async-start | bytes 524288 | tf_op jit(solution)/shard_map/all_to_all | solution.py:111
where the time goes:
time: 97.1 us; the launch traced here: 96.4 us
  blocking collectives  35.8 us (37%)
  matrix products  18.8 us (19%)
  waiting for transfers between devices  16.5 us (17%)
  starting transfers between devices  14.4 us (15%)
  other arithmetic  7.5 us (8%)
  local copies, waits for them, and re-layouts  2.5 us (3%)
    all_gather x1, blocking collectives, per_device(): lax.all_gather(normed, 'ep', axis=0, tiled=True)  23.2 us
    all_to_all x1, blocking collectives, per_device(): lax.all_to_all(outgoing, 'ep', split_axis=0, concat_axis=0, tiled=True)  12.6 us
    all_to_all x1, waiting for transfers between devices, per_device(): lax.all_to_all(expert_out, 'ep', split_axis=0, concat_axis=0, tiled=True)  9.91 us
    dot_general x1, matrix products, per_device(): jnp.einsum('secf,efd->secd', hidden, w_down, preferred_element_type=jnp.f...  8.78 us
    all_to_all x1, starting transfers between devices, per_device(): lax.all_to_all(joined, 'ep', split_axis=1, concat_axis=0, tiled=True)  7.41 us
    all_to_all x1, waiting for transfers between devices, per_device(): lax.all_to_all(all_columns, 'ep', split_axis=0, concat_axis=1, tiled=True)  6.61 us
    dot_general x1, matrix products, per_device(): jnp.einsum('secd,edf->secf', arrived, w_gate_in, preferred_element_type=j...  4.92 us
    all_to_all x1, starting transfers between devices, per_device(): lax.all_to_all(expert_out, 'ep', split_axis=0, concat_axis=0, tiled=True)  3.53 us
  transfers between devices with their start and end apart: 3, of which 2 were waited for; matrix products, arithmetic and copies ran while one was open for 4% of the time, Pallas kernels for 0%

commit v1 on v0

v1 whole, which is shorter than its diff:
```python
import functools

import jax
import jax.numpy as jnp
from jax import lax
from jax.experimental import pallas as pl
from jax.experimental.pallas import tpu as pltpu
from jax.sharding import PartitionSpec as P

CAP = 2
EPS = 1e-06
TAU = 16.0
ALPHA = 1.702
LIMIT = 7.0
MESH = pl.DeviceIdType.MESH
F32 = jnp.float32
BF16 = jnp.bfloat16


def rms_scale(values, gain):
    return values * lax.rsqrt(jnp.mean(values * values, axis=-1, keepdims=True) + EPS) * gain


def dot(a, b):
    return jnp.dot(a, b, preferred_element_type=F32)


def kernel(
    n,
    tokens_ref,
    g_mix_ref,
    wdd_ref,
    wdu_ref,
    bias_ref,
    g_head_ref,
    g_ffn_ref,
    routes_ref,
    scores_ref,
    state_hbm,
    wq_hbm,
    wk_hbm,
    wv_hbm,
    wo_hbm,
    wg_hbm,
    wl_hbm,
    wd_hbm,
    out_ref,
    new_state_hbm,
    wall,
    st,
    wo,
    wg,
    wl,
    wd,
    nsend,
    nrcv,
    psend,
    prcv,
    q_t,
    k_t,
    d_t,
    v_h,
    att,
    headed,
    xs,
    osend,
    orcv,
    hid,
    rsend,
    rrcv,
    local_sem,
    expert_sem,
    w_sem,
    a_send,
    a_recv,
    b_send,
    b_recv,
    o_send,
    o_recv,
    r_send,
    r_recv,
):
    me = lax.axis_index("ep")
    pairs = n // 2
    core = lax.rem(me, 2)
    pair = me // 2
    sibling = me + 1 - 2 * core
    rows, width = tokens_ref.shape
    _, heads, dk, dv = st.shape
    qk = heads * dk
    local_experts, _, ff = wg.shape
    slots = osend.shape[1]
    pair_k = nsend.shape[2]

    barrier = pltpu.get_barrier_semaphore()
    for d in range(1, n):
        pl.semaphore_signal(
            barrier, inc=1, device_id={"ep": lax.rem(me + d, n)}, device_id_type=MESH
        )
    own = wall.at[core]
    proj = [
        pltpu.make_async_copy(wq_hbm, own.at[:, pl.ds(0, qk)], local_sem.at[0]),
        pltpu.make_async_copy(wk_hbm, own.at[:, pl.ds(qk, qk)], local_sem.at[1]),
        pltpu.make_async_copy(wv_hbm, own.at[:, pl.ds(2 * qk, heads * dv)], local_sem.at[2]),
    ]
    for copy in proj:
        copy.start()
    state_in = pltpu.make_async_copy(state_hbm, st, local_sem.at[3])
    wo_in = pltpu.make_async_copy(wo_hbm, wo, local_sem.at[4])
    state_in.start()
    wo_in.start()

    tokens = tokens_ref[...].astype(F32)
    normed = rms_scale(tokens, g_mix_ref[...]).astype(BF16)
    for j in range(pairs):
        nsend[j] = normed[:, j * pair_k : (j + 1) * pair_k]
    for copy in proj:
        copy.wait()
    pl.semaphore_wait(barrier, n - 1)

    w_copy = pltpu.make_async_remote_copy(
        src_ref=own,
        dst_ref=wall.at[core],
        send_sem=w_sem.at[0],
        recv_sem=w_sem.at[1],
        device_id={"ep": sibling},
        device_id_type=MESH,
    )

    def pair_copies(source, target, send, recv):
        copies = []
        for d in range(1, pairs):
            other = lax.rem(pair + d, pairs)
            copies.append(
                pltpu.make_async_remote_copy(
                    src_ref=source.at[other],
                    dst_ref=target.at[pair],
                    send_sem=send.at[d],
                    recv_sem=recv.at[d],
                    device_id={"ep": other * 2 + core},
                    device_id_type=MESH,
                )
            )
        return copies

    def all_copies(source, target, send, recv):
        copies = []
        for d in range(1, n):
            other = lax.rem(me + d, n)
            copies.append(
                pltpu.make_async_remote_copy(
                    src_ref=source.at[other],
                    dst_ref=target.at[me],
                    send_sem=send.at[d],
                    recv_sem=recv.at[d],
                    device_id={"ep": other},
                    device_id_type=MESH,
                )
            )
        return copies

    a_copies = pair_copies(nsend, nrcv, a_send, a_recv)
    for copy in a_copies:
        copy.start()
    w_copy.start()
    gates, lins, downs = [], [], []
    for e in range(local_experts):
        gates.append(pltpu.make_async_copy(wg_hbm.at[e], wg.at[e], expert_sem.at[0, e]))
        lins.append(pltpu.make_async_copy(wl_hbm.at[e], wl.at[e], expert_sem.at[1, e]))
        downs.append(
            pltpu.make_async_copy(wd_hbm.at[e], wd.at[pl.ds(e * ff, ff)], expert_sem.at[2, e])
        )
    for copy in gates + lins + downs:
        copy.start()

    nrcv[pair] = nsend[pair]
    low_rank = dot(normed, wdd_ref[...]).astype(BF16)
    pre = dot(low_rank, wdu_ref[...]) + bias_ref[...]
    log_decay = (jnp.minimum(pre, 0.0) - jnp.log1p(jnp.exp(-jnp.abs(pre)))) / TAU
    d_t[...] = jnp.transpose(jnp.exp(log_decay))

    routes = routes_ref[...]
    scores = scores_ref[...]
    top = routes.shape[1]
    lanes = max(128, n * slots)
    slot = lax.broadcasted_iota(jnp.int32, (rows, lanes), 1)
    slot_expert = slot // CAP
    slot_rank = slot - slot_expert * CAP
    shifted = jnp.exp(scores - jnp.max(scores, axis=-1, keepdims=True))
    weights = shifted / jnp.sum(shifted, axis=-1, keepdims=True)
    named = jnp.zeros((rows, lanes), F32)
    weighted = jnp.zeros((rows, lanes), F32)
    for k in range(top):
        hit = routes[:, k : k + 1] == slot_expert
        named = named + jnp.where(hit, 1.0, 0.0)
        weighted = weighted + jnp.where(hit, weights[:, k : k + 1], 0.0)
    row_index = lax.broadcasted_iota(jnp.int32, (rows, lanes), 0)
    rank = jnp.zeros((rows, lanes), F32)
    for t in range(rows - 1):
        rank = rank + jnp.where(row_index > t, named[t : t + 1, :], 0.0)
    picked = jnp.where(rank == slot_rank.astype(F32), named, 0.0)
    combine = (weighted * picked)[:, : n * slots]
    combine_high = combine.astype(BF16)
    combine_low = (combine - combine_high.astype(F32)).astype(BF16)
    pick_t = jnp.transpose(picked)[: n * slots, :].astype(BF16)

    w_copy.wait()
    for copy in a_copies:
        copy.wait()
    gathered = nrcv[...].astype(F32).reshape(pairs * rows, pair_k).astype(BF16)
    block = 512
    for j in range(width // block):
        part = dot(
            gathered, wall[:, :, j * block : (j + 1) * block].reshape(pair_k, block)
        )
        psend[:, :, j * block : (j + 1) * block] = part.reshape(pairs, rows, block).astype(BF16)
    b_copies = pair_copies(psend, prcv, b_send, b_recv)
    for copy in b_copies:
        copy.start()
    prcv[pair] = psend[pair]
    for copy in b_copies:
        copy.wait()
    summed = prcv[0].astype(F32)
    for j in range(1, pairs):
        summed = summed + prcv[j].astype(F32)
    q_t[...] = jnp.transpose(summed[:, :qk] * dk ** (-0.5))
    k_t[...] = jnp.transpose(summed[:, qk : 2 * qk])
    for h in range(heads):
        v_h[h] = summed[:, 2 * qk + h * dv : 2 * qk + (h + 1) * dv]
    state_in.wait()

    def head_step(h, carry):
        span = pl.ds(pl.multiple_of(h * dk, dk), dk)
        q_block, k_block, d_block = q_t[span, :], k_t[span, :], d_t[span, :]
        v_block = v_h[h]
        for b in range(rows):
            updated = (
                d_block[:, b : b + 1] * st[b, h] + k_block[:, b : b + 1] * v_block[b : b + 1, :]
            )
            st[b, h] = updated
            att[h, pl.ds(b, 1), :] = jnp.sum(q_block[:, b : b + 1] * updated, axis=0, keepdims=True)
        return carry

    lax.fori_loop(0, heads, head_step, 0)
    state_out = pltpu.make_async_copy(st, new_state_hbm, local_sem.at[5])
    state_out.start()
    for h in range(heads):
        headed[:, h * dv : (h + 1) * dv] = rms_scale(att[h], g_head_ref[...]).astype(BF16)
    wo_in.wait()
    mixed = headed[...]
    residual = jnp.concatenate(
        [dot(mixed, wo[:, j * block : (j + 1) * block]) for j in range(width // block)], axis=1
    )
    residual = (tokens + residual).astype(BF16).astype(F32)
    fed = rms_scale(residual, g_ffn_ref[...]).astype(BF16)
    xs[...] = dot(pick_t, fed)
    for j in range(n):
        osend[j] = xs[j * slots : (j + 1) * slots, :].astype(BF16)
    o_copies = all_copies(osend, orcv, o_send, o_recv)
    for copy in o_copies:
        copy.start()
    orcv[me] = osend[me]
    for copy in o_copies:
        copy.wait()
    for j in range(n):
        xs[j * slots : (j + 1) * slots, :] = orcv[j].astype(F32)

    tile = 256
    row_expert = lax.rem(lax.broadcasted_iota(jnp.int32, (n * slots, tile), 0), slots) // CAP
    x = xs[...].astype(BF16)
    for e in range(local_experts):
        gates[e].wait()
        lins[e].wait()

        def up_step(f, carry, e=e):
            span = pl.ds(pl.multiple_of(f * tile, tile), tile)
            gate = jnp.minimum(dot(x, wg[e, :, span]), LIMIT)
            lin = jnp.clip(dot(x, wl[e, :, span]), -LIMIT, LIMIT)
            value = gate * (1.0 / (1.0 + jnp.exp(-ALPHA * gate))) * (lin + 1.0)
            value = jnp.where(row_expert == e, value, 0.0)
            hid[:, pl.ds(pl.multiple_of(e * ff + f * tile, tile), tile)] = value.astype(BF16)
            return carry

        lax.fori_loop(0, ff // tile, up_step, 0)
    for copy in downs:
        copy.wait()
    hidden = hid[...]

    def down_step(f, carry):
        span = pl.ds(pl.multiple_of(f * tile, tile), tile)
        xs[:, span] = dot(hidden, wd[:, span])
        return carry

    lax.fori_loop(0, width // tile, down_step, 0)
    for j in range(n):
        rsend[j] = xs[j * slots : (j + 1) * slots, :].astype(BF16)
    r_copies = all_copies(rsend, rrcv, r_send, r_recv)
    for copy in r_copies:
        copy.start()
    rrcv[me] = rsend[me]
    for copy in r_copies:
        copy.wait()
    for j in range(n):
        xs[j * slots : (j + 1) * slots, :] = rrcv[j].astype(F32)
    returned = xs[...].astype(BF16)
    expert_sum = dot(combine_high, returned) + dot(combine_low, returned)
    out_ref[...] = (residual + expert_sum).astype(BF16)
    state_out.wait()


def per_device(
    n,
    tokens,
    state,
    g_mix,
    w_query,
    w_key,
    w_value,
    w_decay_down,
    w_decay_up,
    decay_bias,
    g_head,
    w_out,
    g_ffn,
    routes,
    route_scores,
    w_gate_in,
    w_lin_in,
    w_down,
):
    rows, width = tokens.shape
    _, heads, dk, dv = state.shape
    qk = heads * dk
    local_experts, _, ff = w_gate_in.shape
    slots = local_experts * CAP
    pairs = n // 2
    kb = w_query.shape[0]
    vmem = pl.BlockSpec(memory_space=pltpu.VMEM)
    hbm = pl.BlockSpec(memory_space=pl.ANY)
    dma = pltpu.SemaphoreType.DMA
    return pl.pallas_call(
        functools.partial(kernel, n),
        out_shape=(
            jax.ShapeDtypeStruct(tokens.shape, BF16),
            jax.ShapeDtypeStruct(state.shape, F32),
        ),
        in_specs=[vmem] * 9 + [hbm] * 8,
        out_specs=(vmem, hbm),
        scratch_shapes=[
            pltpu.VMEM((2, kb, width), BF16),
            pltpu.VMEM(state.shape, F32),
            pltpu.VMEM(w_out.shape, BF16),
            pltpu.VMEM(w_gate_in.shape, BF16),
            pltpu.VMEM(w_lin_in.shape, BF16),
            pltpu.VMEM((local_experts * ff, width), BF16),
            pltpu.VMEM((pairs, rows, 2 * kb), BF16),
            pltpu.VMEM((pairs, rows, 2 * kb), BF16),
            pltpu.VMEM((pairs, rows, width), BF16),
            pltpu.VMEM((pairs, rows, width), BF16),
            pltpu.VMEM((qk, rows), F32),
            pltpu.VMEM((qk, rows), F32),
            pltpu.VMEM((qk, rows), F32),
            pltpu.VMEM((heads, rows, dv), F32),
            pltpu.VMEM((heads, rows, dv), F32),
            pltpu.VMEM((rows, heads * dv), BF16),
            pltpu.VMEM((n * slots, width), F32),
            pltpu.VMEM((n, slots, width), BF16),
            pltpu.VMEM((n, slots, width), BF16),
            pltpu.VMEM((n * slots, local_experts * ff), BF16),
            pltpu.VMEM((n, slots, width), BF16),
            pltpu.VMEM((n, slots, width), BF16),
            dma((6,)),
            dma((3, local_experts)),
            dma((2,)),
            dma((pairs,)),
            dma((pairs,)),
            dma((pairs,)),
            dma((pairs,)),
            dma((n,)),
            dma((n,)),
            dma((n,)),
            dma((n,)),
        ],
        compiler_params=pltpu.CompilerParams(
            collective_id=0, has_side_effects=True, vmem_limit_bytes=60 * 1024 * 1024
        ),
    )(
        tokens,
        g_mix.reshape(1, -1),
        w_decay_down,
        w_decay_up,
        decay_bias.reshape(1, -1),
        g_head.reshape(1, -1),
        g_ffn.reshape(1, -1),
        routes,
        route_scores,
        state,
        w_query,
        w_key,
        w_value,
        w_out,
        w_gate_in,
        w_lin_in,
        w_down,
    )


def solution(mesh):
    return jax.shard_map(
        functools.partial(per_device, mesh.shape["ep"]),
        mesh=mesh,
        in_specs=(
            P(("grp", "ep"), None),
            P(("grp", "ep"), None, None, None),
            P(),
            P("ep", None),
            P("ep", None),
            P("ep", None),
            P(),
            P(),
            P(),
            P(),
            P(),
            P(),
            P(("grp", "ep"), None),
            P(("grp", "ep"), None),
            P("ep", None, None),
            P("ep", None, None),
            P("ep", None, None),
        ),
        out_specs=(P(("grp", "ep"), None), P(("grp", "ep"), None, None, None)),
        check_vma=False,
    )
```

time: 97.1 us -> 51.3 us (0.53)
  Pallas kernels: 0 us -> 40.8 us
  blocking collectives: 35.8 us -> 0 us
  matrix products: 18.8 us -> 0 us
  waiting for transfers between devices: 16.5 us -> 0 us
  starting transfers between devices: 14.4 us -> 0 us
  other arithmetic: 7.5 us -> 0 us
  local copies, waits for them, and re-layouts: 2.5 us -> 9.13 us
    pallas_call x0 -> x1, Pallas kernels: none -> 40.8 us  [per_device(): pl.pallas_call(functools.partial(kernel, n), out_shape=(jax.ShapeDtypeStr...]
    all_gather x1 -> x0, blocking collectives: 23.2 us -> none  [per_device(): lax.all_gather(normed, 'ep', axis=0, tiled=True)]
    dot_general x8 -> x0, matrix products: 18.8 us -> none  [the longest x1 8.78 us: per_device(): jnp.einsum('secf,efd->secd', hidden, w_down, preferred_element_type=jnp.f...]
    all_to_all x3 -> x0, waiting for transfers between devices: 16.5 us -> none  [the longest x1 9.91 us: per_device(): lax.all_to_all(expert_out, 'ep', split_axis=0, concat_axis=0, tiled=True)]
    all_to_all x3 -> x0, starting transfers between devices: 14.4 us -> none  [the longest x1 7.41 us: per_device(): lax.all_to_all(joined, 'ep', split_axis=1, concat_axis=0, tiled=True)]
    all_to_all x1 -> x0, blocking collectives: 12.6 us -> none  [per_device(): lax.all_to_all(outgoing, 'ep', split_axis=0, concat_axis=0, tiled=True)]
    unnamed x17 -> x5, local copies, waits for them, and re-layouts: 0.82 us -> 9.13 us
    add x2 -> x0, other arithmetic: 2.62 us -> none  [the longest x1 2.61 us: per_device(): jnp.exp(log_decay)[..., None] * state]
  transfers between devices with their start and end apart: 3 -> 0, of which waited for: 2 -> 0; matrix products, arithmetic and copies ran while one was open for 4% -> 0% of each run, Pallas kernels for 0% -> 0%
where the time goes in v1:
time: 51.3 us; the launch traced here: 50.6 us
  Pallas kernels  40.8 us (80%)
  local copies, waits for them, and re-layouts  9.13 us (18%)
  between operations  0.64 us (1%)
    pallas_call x1, Pallas kernels, per_device(): pl.pallas_call(functools.partial(kernel, n), out_shape=(jax.ShapeDtypeStr...  40.8 us
    unnamed x5, local copies, waits for them, and re-layouts  9.13 us

profile of v1, /device:TPU:0, one launch (start us, length us, event | category | flops | bytes accessed | tf_op | source)
XLA Modules:
  0.0 50.6 jit_solution(11911496741670689734)
XLA Ops:
  0.6 1.3 %copy.20.routes_ref = s32[8,4]{1,0:T(8,128)} copy(s32[8,4]{0,1:T(4,128)} %param.29) | data formatting | bytes 256 | tf_op args[12]
  2.0 1.3 %copy.21.scores_ref = f32[8,4]{1,0:T(8,128)} copy(f32[8,4]{0,1:T(4,128)} %param.30) | data formatting | bytes 256 | tf_op args[13]
  3.3 1.9 %copy.19.wdd_ref = bf16[2048,32]{1,0:T(8,128)(2,1)} copy(bf16[2048,32]{0,1:T(8,128)(2,1)} %param.23) | data formatting | bytes 262144 | tf_op args[6]
  5.2 40.8 %shard_map.176 = (bf16[8,2048]{1,0:T(8,128)(2,1)}, f32[8,8,64,128]{3,2,1,0:T(8,128)}) custom-call(bf16[8,2048]{1,0:T(8,128)(2,1)} %tokens_ref.1, f32[1,2048]{1,0:T(1,128)} %bitcast.4, bf16[2048,32]{1,0:T(8,128)(2,1)} %copy.19.wdd_ref, bf16[32,512]{1,0:T(8,128)(2,1)} %wdu_ref.1, f32[1,512]{1,0:T(1,128)} %bitcast.6, f32[1,128]{1,0:T(1,128)} %bitcast.7, ...), custom_call_target="tpu_custom_call" | custom-call | tf_op jit(solution)/shard_map/pallas_call | solution.py:341
  46.1 1.4 %copy.24 = bf16[8,2048]{1,0:T(8,128)(2,1)} copy(bf16[8,2048]{1,0:T(8,128)(2,1)} %get-tuple-element.4) | data formatting | bytes 65536
  47.4 3.2 %copy.25 = f32[8,8,64,128]{3,2,1,0:T(8,128)} copy(f32[8,8,64,128]{3,2,1,0:T(8,128)} %get-tuple-element.5) | data formatting | bytes 4194304

commit v2 on v1

--- a/solution.py
+++ b/solution.py
@@ -45,7 +45,9 @@
     wl_hbm,
     wd_hbm,
     out_ref,
-    new_state_hbm,
+    k_t,
+    d_t,
+    v_h,
     wall,
     st,
     wo,
@@ -57,9 +59,6 @@
     psend,
     prcv,
     q_t,
-    k_t,
-    d_t,
-    v_h,
     att,
     headed,
     xs,
@@ -174,35 +173,37 @@
         copy.start()
 
     nrcv[pair] = nsend[pair]
-    low_rank = dot(normed, wdd_ref[...]).astype(BF16)
+    low_rank = lax.dot_general(
+        normed, wdd_ref[...], (((1,), (1,)), ((), ())), preferred_element_type=F32
+    ).astype(BF16)
     pre = dot(low_rank, wdu_ref[...]) + bias_ref[...]
     log_decay = (jnp.minimum(pre, 0.0) - jnp.log1p(jnp.exp(-jnp.abs(pre)))) / TAU
     d_t[...] = jnp.transpose(jnp.exp(log_decay))
 
     routes = routes_ref[...]
     scores = scores_ref[...]
-    top = routes.shape[1]
-    lanes = max(128, n * slots)
-    slot = lax.broadcasted_iota(jnp.int32, (rows, lanes), 1)
-    slot_expert = slot // CAP
-    slot_rank = slot - slot_expert * CAP
-    shifted = jnp.exp(scores - jnp.max(scores, axis=-1, keepdims=True))
-    weights = shifted / jnp.sum(shifted, axis=-1, keepdims=True)
-    named = jnp.zeros((rows, lanes), F32)
-    weighted = jnp.zeros((rows, lanes), F32)
+    top = routes.shape[0]
+    spots = n * slots
+    spot = lax.broadcasted_iota(jnp.int32, (spots, rows), 0)
+    spot_expert = spot // CAP
+    spot_rank = (spot - spot_expert * CAP).astype(F32)
+    shifted = jnp.exp(scores - jnp.max(scores, axis=0, keepdims=True))
+    weights = shifted / jnp.sum(shifted, axis=0, keepdims=True)
+    named = jnp.zeros((spots, rows), F32)
+    weighted = jnp.zeros((spots, rows), F32)
     for k in range(top):
-        hit = routes[:, k : k + 1] == slot_expert
+        hit = routes[k : k + 1, :] == spot_expert
         named = named + jnp.where(hit, 1.0, 0.0)
-        weighted = weighted + jnp.where(hit, weights[:, k : k + 1], 0.0)
-    row_index = lax.broadcasted_iota(jnp.int32, (rows, lanes), 0)
-    rank = jnp.zeros((rows, lanes), F32)
+        weighted = weighted + jnp.where(hit, weights[k : k + 1, :], 0.0)
+    token = lax.broadcasted_iota(jnp.int32, (spots, rows), 1)
+    rank = jnp.zeros((spots, rows), F32)
     for t in range(rows - 1):
-        rank = rank + jnp.where(row_index > t, named[t : t + 1, :], 0.0)
-    picked = jnp.where(rank == slot_rank.astype(F32), named, 0.0)
-    combine = (weighted * picked)[:, : n * slots]
+        rank = rank + jnp.where(token > t, named[:, t : t + 1], 0.0)
+    picked = jnp.where(rank == spot_rank, named, 0.0)
+    combine = jnp.transpose(weighted * picked)
     combine_high = combine.astype(BF16)
     combine_low = (combine - combine_high.astype(F32)).astype(BF16)
-    pick_t = jnp.transpose(picked)[: n * slots, :].astype(BF16)
+    pick_t = picked.astype(BF16)
 
     w_copy.wait()
     for copy in a_copies:
@@ -218,6 +219,15 @@
     for copy in b_copies:
         copy.start()
     prcv[pair] = psend[pair]
+    state_in.wait()
+
+    def decay_step(h, carry):
+        d_block = d_t[pl.ds(pl.multiple_of(h * dk, dk), dk), :]
+        for b in range(rows):
+            st[b, h] = d_block[:, b : b + 1] * st[b, h]
+        return carry
+
+    lax.fori_loop(0, heads, decay_step, 0)
     for copy in b_copies:
         copy.wait()
     summed = prcv[0].astype(F32)
@@ -227,25 +237,22 @@
     k_t[...] = jnp.transpose(summed[:, qk : 2 * qk])
     for h in range(heads):
         v_h[h] = summed[:, 2 * qk + h * dv : 2 * qk + (h + 1) * dv]
-    state_in.wait()
 
     def head_step(h, carry):
-        span = pl.ds(pl.multiple_of(h * dk, dk), dk)
-        q_block, k_block, d_block = q_t[span, :], k_t[span, :], d_t[span, :]
-        v_block = v_h[h]
+        q_block = q_t[pl.ds(pl.multiple_of(h * dk, dk), dk), :]
         for b in range(rows):
-            updated = (
-                d_block[:, b : b + 1] * st[b, h] + k_block[:, b : b + 1] * v_block[b : b + 1, :]
+            att[h, pl.ds(b, 1), :] = jnp.sum(
+                q_block[:, b : b + 1] * st[b, h], axis=0, keepdims=True
             )
-            st[b, h] = updated
-            att[h, pl.ds(b, 1), :] = jnp.sum(q_block[:, b : b + 1] * updated, axis=0, keepdims=True)
         return carry
 
     lax.fori_loop(0, heads, head_step, 0)
-    state_out = pltpu.make_async_copy(st, new_state_hbm, local_sem.at[5])
-    state_out.start()
+    query_key = summed[:, :qk] * dk ** (-0.5) * summed[:, qk : 2 * qk]
     for h in range(heads):
-        headed[:, h * dv : (h + 1) * dv] = rms_scale(att[h], g_head_ref[...]).astype(BF16)
+        score = jnp.sum(query_key[:, h * dk : (h + 1) * dk], axis=1, keepdims=True)
+        headed[:, h * dv : (h + 1) * dv] = rms_scale(
+            att[h] + score * v_h[h], g_head_ref[...]
+        ).astype(BF16)
     wo_in.wait()
     mixed = headed[...]
     residual = jnp.concatenate(
@@ -305,7 +312,28 @@
     returned = xs[...].astype(BF16)
     expert_sum = dot(combine_high, returned) + dot(combine_low, returned)
     out_ref[...] = (residual + expert_sum).astype(BF16)
-    state_out.wait()
+
+
+def finish(layer_ref, k_ref, d_ref, v_ref, state_hbm, out_ref, new_state_hbm, st, in_sem, out_sem):
+    rows, heads, dk, _ = st.shape
+    ins = [pltpu.make_async_copy(state_hbm.at[b], st.at[b], in_sem.at[b]) for b in range(rows)]
+    outs = [pltpu.make_async_copy(st.at[b], new_state_hbm.at[b], out_sem.at[b]) for b in range(rows)]
+    for copy in ins:
+        copy.start()
+    out_ref[...] = layer_ref[...]
+    for b in range(rows):
+        ins[b].wait()
+
+        def head_step(h, carry, b=b):
+            span = pl.ds(pl.multiple_of(h * dk, dk), dk)
+            k_block, d_block = k_ref[span, b : b + 1], d_ref[span, b : b + 1]
+            st[b, h] = d_block * st[b, h] + k_block * v_ref[h, b : b + 1, :]
+            return carry
+
+        lax.fori_loop(0, heads, head_step, 0, unroll=True)
+        outs[b].start()
+    for copy in outs:
+        copy.wait()
 
 
 def per_device(
@@ -338,14 +366,16 @@
     vmem = pl.BlockSpec(memory_space=pltpu.VMEM)
     hbm = pl.BlockSpec(memory_space=pl.ANY)
     dma = pltpu.SemaphoreType.DMA
-    return pl.pallas_call(
+    layer, keys, decays, values = pl.pallas_call(
         functools.partial(kernel, n),
         out_shape=(
             jax.ShapeDtypeStruct(tokens.shape, BF16),
-            jax.ShapeDtypeStruct(state.shape, F32),
+            jax.ShapeDtypeStruct((qk, rows), F32),
+            jax.ShapeDtypeStruct((qk, rows), F32),
+            jax.ShapeDtypeStruct((heads, rows, dv), F32),
         ),
         in_specs=[vmem] * 9 + [hbm] * 8,
-        out_specs=(vmem, hbm),
+        out_specs=(vmem,) * 4,
         scratch_shapes=[
             pltpu.VMEM((2, kb, width), BF16),
             pltpu.VMEM(state.shape, F32),
@@ -358,9 +388,6 @@
             pltpu.VMEM((pairs, rows, width), BF16),
             pltpu.VMEM((pairs, rows, width), BF16),
             pltpu.VMEM((qk, rows), F32),
-            pltpu.VMEM((qk, rows), F32),
-            pltpu.VMEM((qk, rows), F32),
-            pltpu.VMEM((heads, rows, dv), F32),
             pltpu.VMEM((heads, rows, dv), F32),
             pltpu.VMEM((rows, heads * dv), BF16),
             pltpu.VMEM((n * slots, width), F32),
@@ -387,13 +414,13 @@
     )(
         tokens,
         g_mix.reshape(1, -1),
-        w_decay_down,
+        w_decay_down.T,
         w_decay_up,
         decay_bias.reshape(1, -1),
         g_head.reshape(1, -1),
         g_ffn.reshape(1, -1),
-        routes,
-        route_scores,
+        routes.T,
+        route_scores.T,
         state,
         w_query,
         w_key,
@@ -403,6 +430,16 @@
         w_lin_in,
         w_down,
     )
+    return pl.pallas_call(
+        finish,
+        out_shape=(
+            jax.ShapeDtypeStruct(tokens.shape, BF16),
+            jax.ShapeDtypeStruct(state.shape, F32),
+        ),
+        in_specs=[vmem] * 4 + [hbm],
+        out_specs=(vmem, hbm),
+        scratch_shapes=[pltpu.VMEM(state.shape, F32), dma((rows,)), dma((rows,))],
+    )(layer, keys, decays, values, state)
 
 
 def solution(mesh):

time: 51.3 us -> 46.1 us (0.90)
  local copies, waits for them, and re-layouts: 9.13 us -> 0 us
  Pallas kernels: 40.8 us -> 44.9 us
    unnamed x5 -> x0, local copies, waits for them, and re-layouts: 9.13 us -> none
    pallas_call x0 -> x1, Pallas kernels: none -> 5.1 us  [per_device(): pl.pallas_call(finish, out_shape=(jax.ShapeDtypeStruct(tokens.shape, BF16...]
    pallas_call x1, Pallas kernels: 40.8 us -> 39.8 us  [per_device(): pl.pallas_call(functools.partial(kernel, n), out_shape=(jax.ShapeDtypeStr...]
where the time goes in v2:
time: 46.1 us; the launch traced here: 45.5 us
  Pallas kernels  44.9 us (97%)
  between operations  0.64 us (1%)
    pallas_call x1, Pallas kernels, per_device(): pl.pallas_call(functools.partial(kernel, n), out_shape=(jax.ShapeDtypeStr...  39.8 us
    pallas_call x1, Pallas kernels, per_device(): pl.pallas_call(finish, out_shape=(jax.ShapeDtypeStruct(tokens.shape, BF16...  5.1 us

profile of v2, /device:TPU:0, one launch (start us, length us, event | category | flops | bytes accessed | tf_op | source)
XLA Modules:
  0.0 45.5 jit_solution(9781081412808860418)
XLA Ops:
  0.6 39.8 %shard_map.176 = (bf16[8,2048]{1,0:T(8,128)(2,1)}, f32[512,8]{1,0:T(8,128)}, f32[512,8]{1,0:T(8,128)}, f32[8,8,128]{2,1,0:T(8,128)}) custom-call(bf16[8,2048]{1,0:T(8,128)(2,1)} %tokens_ref.1, f32[1,2048]{1,0:T(1,128)} %bitcast.8, bf16[32,2048]{1,0:T(8,128)(2,1)} %bitcast.7, bf16[32,512]{1,0:T(8,128)(2,1)} %wdu_ref.1, f32[1,512]{1,0:T(1,128)} %bitcast.10, ...), custom_call_target="tpu_custom_call" | custom-call | tf_op jit(solution)/shard_map/pallas_call | solution.py:369
  40.4 5.1 %shard_map.177 = (bf16[8,2048]{1,0:T(8,128)(2,1)}, f32[8,8,64,128]{3,2,1,0:T(8,128)}) custom-call(bf16[8,2048]{1,0:T(8,128)(2,1)} %get-tuple-element.6.layer_ref, f32[512,8]{1,0:T(8,128)} %get-tuple-element.7.k_ref, f32[512,8]{1,0:T(8,128)} %get-tuple-element.8.d_ref, f32[8,8,128]{2,1,0:T(8,128)} %get-tuple-element.9.v_ref, f32[8,8,64,128]{3,2,1,0:T(8,128)} %state_hbm.3), custom_call_target="tpu_custom_call" | custom-call | tf_op jit(solution)/shard_map/pallas_call | solution.py:433

commit v3 on v2

--- a/solution.py
+++ b/solution.py
@@ -45,9 +45,9 @@
     wl_hbm,
     wd_hbm,
     out_ref,
-    k_t,
-    d_t,
-    v_h,
+    k_ref,
+    d_ref,
+    v_ref,
     wall,
     st,
     wo,
@@ -58,7 +58,8 @@
     nrcv,
     psend,
     prcv,
-    q_t,
+    st_high,
+    st_low,
     att,
     headed,
     xs,
@@ -178,7 +179,8 @@
     ).astype(BF16)
     pre = dot(low_rank, wdu_ref[...]) + bias_ref[...]
     log_decay = (jnp.minimum(pre, 0.0) - jnp.log1p(jnp.exp(-jnp.abs(pre)))) / TAU
-    d_t[...] = jnp.transpose(jnp.exp(log_decay))
+    decay = jnp.exp(log_decay)
+    d_ref[...] = decay
 
     routes = routes_ref[...]
     scores = scores_ref[...]
@@ -221,37 +223,39 @@
     prcv[pair] = psend[pair]
     state_in.wait()
 
-    def decay_step(h, carry):
-        d_block = d_t[pl.ds(pl.multiple_of(h * dk, dk), dk), :]
-        for b in range(rows):
-            st[b, h] = d_block[:, b : b + 1] * st[b, h]
+    def split_step(b, carry):
+        part = st[b].reshape(qk, dv)
+        high = part.astype(BF16)
+        st_high[b] = high
+        st_low[b] = (part - high.astype(F32)).astype(BF16)
         return carry
 
-    lax.fori_loop(0, heads, decay_step, 0)
+    lax.fori_loop(0, rows, split_step, 0)
     for copy in b_copies:
         copy.wait()
     summed = prcv[0].astype(F32)
     for j in range(1, pairs):
         summed = summed + prcv[j].astype(F32)
-    q_t[...] = jnp.transpose(summed[:, :qk] * dk ** (-0.5))
-    k_t[...] = jnp.transpose(summed[:, qk : 2 * qk])
-    for h in range(heads):
-        v_h[h] = summed[:, 2 * qk + h * dv : 2 * qk + (h + 1) * dv]
-
-    def head_step(h, carry):
-        q_block = q_t[pl.ds(pl.multiple_of(h * dk, dk), dk), :]
-        for b in range(rows):
-            att[h, pl.ds(b, 1), :] = jnp.sum(
-                q_block[:, b : b + 1] * st[b, h], axis=0, keepdims=True
-            )
-        return carry
-
-    lax.fori_loop(0, heads, head_step, 0)
-    query_key = summed[:, :qk] * dk ** (-0.5) * summed[:, qk : 2 * qk]
+    queries = summed[:, :qk] * dk ** (-0.5)
+    keys = summed[:, qk : 2 * qk]
+    k_ref[...] = keys
+    v_ref[...] = summed[:, 2 * qk :]
+    reads = queries * decay
+    head_row = lax.broadcasted_iota(jnp.int32, (heads, qk), 0)
+    head_lane = lax.broadcasted_iota(jnp.int32, (heads, qk), 1) // dk
+    for b in range(rows):
+        spread = jnp.where(head_row == head_lane, reads[b : b + 1, :], 0.0)
+        high = spread.astype(BF16)
+        low = (spread - high.astype(F32)).astype(BF16)
+        read = dot(high, st_high[b]) + (dot(low, st_high[b]) + dot(high, st_low[b]))
+        for h in range(heads):
+            att[h, b : b + 1, :] = read[h : h + 1, :]
+    query_key = queries * keys
     for h in range(heads):
         score = jnp.sum(query_key[:, h * dk : (h + 1) * dk], axis=1, keepdims=True)
+        value = summed[:, 2 * qk + h * dv : 2 * qk + (h + 1) * dv]
         headed[:, h * dv : (h + 1) * dv] = rms_scale(
-            att[h] + score * v_h[h], g_head_ref[...]
+            att[h] + score * value, g_head_ref[...]
         ).astype(BF16)
     wo_in.wait()
     mixed = headed[...]
@@ -298,39 +302,55 @@
         xs[:, span] = dot(hidden, wd[:, span])
         return carry
 
-    lax.fori_loop(0, width // tile, down_step, 0)
-    for j in range(n):
-        rsend[j] = xs[j * slots : (j + 1) * slots, :].astype(BF16)
-    r_copies = all_copies(rsend, rrcv, r_send, r_recv)
-    for copy in r_copies:
-        copy.start()
-    rrcv[me] = rsend[me]
-    for copy in r_copies:
-        copy.wait()
-    for j in range(n):
-        xs[j * slots : (j + 1) * slots, :] = rrcv[j].astype(F32)
+    half = width // 2
+    r_copies = []
+    for part in range(2):
+        steps = half // tile
+        lax.fori_loop(part * steps, (part + 1) * steps, down_step, 0)
+        for j in range(n):
+            rsend[part, j] = xs[
+                j * slots : (j + 1) * slots, part * half : (part + 1) * half
+            ].astype(BF16)
+        copies = all_copies(rsend.at[part], rrcv.at[part], r_send.at[part], r_recv.at[part])
+        for copy in copies:
+            copy.start()
+        rrcv[part, me] = rsend[part, me]
+        r_copies.append(copies)
+    for part in range(2):
+        for copy in r_copies[part]:
+            copy.wait()
+        for j in range(n):
+            xs[j * slots : (j + 1) * slots, part * half : (part + 1) * half] = rrcv[
+                part, j
+            ].astype(F32)
     returned = xs[...].astype(BF16)
     expert_sum = dot(combine_high, returned) + dot(combine_low, returned)
     out_ref[...] = (residual + expert_sum).astype(BF16)
 
 
 def finish(layer_ref, k_ref, d_ref, v_ref, state_hbm, out_ref, new_state_hbm, st, in_sem, out_sem):
-    rows, heads, dk, _ = st.shape
+    rows, heads, dk, dv = st.shape
     ins = [pltpu.make_async_copy(state_hbm.at[b], st.at[b], in_sem.at[b]) for b in range(rows)]
     outs = [pltpu.make_async_copy(st.at[b], new_state_hbm.at[b], out_sem.at[b]) for b in range(rows)]
     for copy in ins:
         copy.start()
     out_ref[...] = layer_ref[...]
+    parts = []
+    for ref in (d_ref, k_ref):
+        high = ref[...].astype(BF16).astype(F32)
+        parts += [high, ref[...] - high]
+    columns = jnp.transpose(jnp.concatenate(parts, axis=0)).astype(BF16)
+    shape = (4 * rows, 2 * dv)
+    part_row = lax.broadcasted_iota(jnp.int32, shape, 0)
+    same_kind = (part_row < 2 * rows) == (lax.broadcasted_iota(jnp.int32, shape, 1) < dv)
     for b in range(rows):
+        chosen = same_kind & (lax.rem(part_row, rows) == b)
+        spread = dot(columns, jnp.where(chosen, 1.0, 0.0).astype(BF16))
         ins[b].wait()
-
-        def head_step(h, carry, b=b):
-            span = pl.ds(pl.multiple_of(h * dk, dk), dk)
-            k_block, d_block = k_ref[span, b : b + 1], d_ref[span, b : b + 1]
-            st[b, h] = d_block * st[b, h] + k_block * v_ref[h, b : b + 1, :]
-            return carry
-
-        lax.fori_loop(0, heads, head_step, 0, unroll=True)
+        for h in range(heads):
+            span = slice(h * dk, (h + 1) * dk)
+            value = v_ref[b : b + 1, h * dv : (h + 1) * dv]
+            st[b, h] = spread[span, :dv] * st[b, h] + spread[span, dv:] * value
         outs[b].start()
     for copy in outs:
         copy.wait()
@@ -370,9 +390,9 @@
         functools.partial(kernel, n),
         out_shape=(
             jax.ShapeDtypeStruct(tokens.shape, BF16),
-            jax.ShapeDtypeStruct((qk, rows), F32),
-            jax.ShapeDtypeStruct((qk, rows), F32),
-            jax.ShapeDtypeStruct((heads, rows, dv), F32),
+            jax.ShapeDtypeStruct((rows, qk), F32),
+            jax.ShapeDtypeStruct((rows, qk), F32),
+            jax.ShapeDtypeStruct((rows, heads * dv), F32),
         ),
         in_specs=[vmem] * 9 + [hbm] * 8,
         out_specs=(vmem,) * 4,
@@ -387,15 +407,16 @@
             pltpu.VMEM((pairs, rows, 2 * kb), BF16),
             pltpu.VMEM((pairs, rows, width), BF16),
             pltpu.VMEM((pairs, rows, width), BF16),
-            pltpu.VMEM((qk, rows), F32),
+            pltpu.VMEM((rows, qk, dv), BF16),
+            pltpu.VMEM((rows, qk, dv), BF16),
             pltpu.VMEM((heads, rows, dv), F32),
             pltpu.VMEM((rows, heads * dv), BF16),
             pltpu.VMEM((n * slots, width), F32),
             pltpu.VMEM((n, slots, width), BF16),
             pltpu.VMEM((n, slots, width), BF16),
             pltpu.VMEM((n * slots, local_experts * ff), BF16),
-            pltpu.VMEM((n, slots, width), BF16),
-            pltpu.VMEM((n, slots, width), BF16),
+            pltpu.VMEM((2, n, slots, width // 2), BF16),
+            pltpu.VMEM((2, n, slots, width // 2), BF16),
             dma((6,)),
             dma((3, local_experts)),
             dma((2,)),
@@ -405,8 +426,8 @@
             dma((pairs,)),
             dma((n,)),
             dma((n,)),
-            dma((n,)),
-            dma((n,)),
+            dma((2, n)),
+            dma((2, n)),
         ],
         compiler_params=pltpu.CompilerParams(
             collective_id=0, has_side_effects=True, vmem_limit_bytes=60 * 1024 * 1024

time: 46.1 us -> 45.4 us (0.985)
  no operation moved by 1% of the time
where the time goes in v3:
time: 45.4 us; the launch traced here: 45.1 us
  Pallas kernels  44.5 us (98%)
  between operations  0.64 us (1%)
    pallas_call x1, Pallas kernels, per_device(): pl.pallas_call(functools.partial(kernel, n), out_shape=(jax.ShapeDtypeStr...  39.5 us
    pallas_call x1, Pallas kernels, per_device(): pl.pallas_call(finish, out_shape=(jax.ShapeDtypeStruct(tokens.shape, BF16...  5.04 us

profile of v3, /device:TPU:0, one launch (start us, length us, event | category | flops | bytes accessed | tf_op | source)
XLA Modules:
  0.0 45.1 jit_solution(15422069409255993454)
XLA Ops:
  0.6 39.5 %shard_map.176 = (bf16[8,2048]{1,0:T(8,128)(2,1)}, f32[8,512]{1,0:T(8,128)}, f32[8,512]{1,0:T(8,128)}, f32[8,1024]{1,0:T(8,128)}) custom-call(bf16[8,2048]{1,0:T(8,128)(2,1)} %tokens_ref.1, f32[1,2048]{1,0:T(1,128)} %bitcast.8, bf16[32,2048]{1,0:T(8,128)(2,1)} %bitcast.7, bf16[32,512]{1,0:T(8,128)(2,1)} %wdu_ref.1, f32[1,512]{1,0:T(1,128)} %bitcast.10, ...), custom_call_target="tpu_custom_call" | custom-call | tf_op jit(solution)/shard_map/pallas_call | solution.py:389
  40.1 5.0 %shard_map.177 = (bf16[8,2048]{1,0:T(8,128)(2,1)}, f32[8,8,64,128]{3,2,1,0:T(8,128)}) custom-call(bf16[8,2048]{1,0:T(8,128)(2,1)} %get-tuple-element.6.layer_ref, f32[8,512]{1,0:T(8,128)} %get-tuple-element.7.k_ref, f32[8,512]{1,0:T(8,128)} %get-tuple-element.8.d_ref, f32[8,1024]{1,0:T(8,128)} %get-tuple-element.9.v_ref, f32[8,8,64,128]{3,2,1,0:T(8,128)} %state_hbm.3), custom_call_target="tpu_custom_call" | custom-call | tf_op jit(solution)/shard_map/pallas_call | solution.py:454
